TPU v7x, 32 devices: a whole 2x2x4 slice. The times are simulated.
32 devices in a mesh: ep: 8 (over z, x), tp: 4 (over y, core).
Axes of the slice: x: 2, y: 2, z: 4, core: 2. Of those that a mesh axis runs over, the one named last changes fastest.
Arguments:
- conv_gate: bfloat16 [4096, 2048], P('ep', 'tp'), may hold values from -6 to 6
- conv_in_gate: bfloat16 [4096, 2048], P('ep', 'tp'), may hold values from -6 to 6
- conv_value: bfloat16 [4096, 2048], P('ep', 'tp'), may hold values from -6 to 6
- conv_taps: float32 [3, 2048], P(None, 'tp'), may hold values from -3.5 to 3.5
- mix_out_weight: bfloat16 [2048, 4096], P(None, 'tp'), may hold values from -0.125 to 0.125
- expert_input: bfloat16 [1280, 4096], P('ep', 'tp'), may hold values from -1600 to 1600
- expert_gain: float32 [4096], replicated, may hold values from 0.1 to 1.9
- routes: int32 [1280, 2], P('ep'), may hold values from 0 to 7, all different within a row; in each aligned block of 160 rows (0 to 159, 160 to 319, ...) at most 60 rows name the same one
- group_prob: float32 [1280], P('ep'), may hold values from 0.3 to 1
- pair_logits: float32 [1280, 2], P('ep'), may hold values from -6 to 6
- expert_gate: bfloat16 [8, 4096, 2048], P('ep', None, 'tp'), may hold values from -0.09375 to 0.09375
- expert_up: bfloat16 [8, 4096, 2048], P('ep', None, 'tp'), may hold values from -0.09375 to 0.09375
- expert_down: bfloat16 [8, 2048, 4096], P('ep', None, 'tp'), may hold values from -0.125 to 0.125
Outputs:
- mixed: bfloat16 [4096, 4096], P('ep', 'tp')
- expert_output: bfloat16 [1280, 4096], P('ep', 'tp')
Inputs may be any that keep to these rules, and one draw needn't show every extreme that they name: `routes`: in the 160 rows of one index of ep no expert is named by more than 60 rows, a bound that some block reaches; each row names 2 different experts.
All inputs are finite; a program needn't handle non-finite values.
Results may differ from a plain program's by a relative error of at most 0.0071.
Values may be sent and summed in bfloat16 or wider, within the bound.
No kernel may reach another device: no remote copies, remote signals or barrier semaphores. Data moves between devices by JAX's collectives and lax.ppermute only.
A program may use at most 64 MiB of HBM per device.

v0:
```python
import jax
import jax.numpy as jnp
from jax import lax
from jax.sharding import PartitionSpec as P

D = 4096


EPS = 1e-06


def shifted(block, axis, distance):
    devices = range(lax.axis_size(axis))
    route = [(i - distance, i) for i in devices if i - distance in devices]
    return lax.ppermute(block, axis, route)


def slot_table(route_block, capacity, expert_count):
    pair_ids = route_block.reshape(-1)
    onehot = (pair_ids[:, None] == jnp.arange(expert_count, dtype=jnp.int32)[None, :]).astype(
        jnp.int32
    )
    earlier = jnp.cumsum(onehot, axis=0) - onehot
    within = jnp.sum(earlier * onehot, axis=1)
    return pair_ids * capacity + within


def pair_weights(group_prob, pair_logits):
    spread = pair_logits[:, 0] - pair_logits[:, 1]
    return (
        jnp.stack([jax.nn.sigmoid(spread), jax.nn.sigmoid(-spread)], axis=1) * group_prob[:, None]
    )


def per_device(
    conv_gate,
    conv_in_gate,
    conv_value,
    conv_taps,
    mix_out_weight,
    expert_input,
    expert_gain,
    routes,
    group_prob,
    pair_logits,
    expert_gate,
    expert_up,
    expert_down,
):
    reach = conv_taps.shape[0] - 1
    token_rows = conv_value.shape[0]
    products = conv_in_gate.astype(jnp.float32) * conv_value.astype(jnp.float32)
    earlier_rows = shifted(products[token_rows - reach :], "ep", 1)
    padded = jnp.concatenate([earlier_rows, products], axis=0)
    convolved = jnp.zeros_like(products)
    for offset in range(reach + 1):
        convolved = convolved + conv_taps[offset][None, :] * padded[offset : offset + token_rows]
    mixer_rows = (conv_gate.astype(jnp.float32) * convolved).astype(jnp.bfloat16)
    mixed = jnp.dot(
        lax.all_gather(mixer_rows, "tp", axis=1, tiled=True),
        mix_out_weight,
        preferred_element_type=jnp.float32,
    ).astype(jnp.bfloat16)
    expert_count = lax.axis_size("ep")
    tok_rows, choose_count = routes.shape
    capacity = 3 * tok_rows * choose_count // (2 * expert_count)
    slot_index = slot_table(routes, capacity, expert_count)
    pair_row = jnp.arange(tok_rows * choose_count, dtype=jnp.int32) // choose_count
    slot_rows = expert_count * capacity
    gate_block = expert_gate[0]
    up_block = expert_up[0]
    down_block = expert_down[0]
    columns = expert_input.shape[1]
    features = expert_input.astype(jnp.float32)
    squares = lax.psum(jnp.sum(features * features, axis=1), "tp")
    scale = lax.rsqrt(squares / D + EPS)
    gain_part = lax.dynamic_slice_in_dim(expert_gain, lax.axis_index("tp") * columns, columns, 0)
    normed = (features * scale[:, None] * gain_part[None, :]).astype(jnp.bfloat16)
    buffer = jnp.zeros((slot_rows, columns), jnp.bfloat16).at[slot_index].set(normed[pair_row])
    arrived = lax.all_to_all(
        buffer.reshape(expert_count, capacity, columns),
        "ep",
        split_axis=0,
        concat_axis=0,
        tiled=True,
    ).reshape(slot_rows, columns)
    shard_piece = lax.all_gather(arrived, "tp", axis=1, tiled=True)
    gate_sum = jnp.dot(shard_piece, gate_block, preferred_element_type=jnp.float32)
    up_sum = jnp.dot(shard_piece, up_block, preferred_element_type=jnp.float32)
    hidden = (jax.nn.silu(gate_sum) * up_sum).astype(jnp.bfloat16)
    results = jnp.dot(
        lax.all_gather(hidden, "tp", axis=1, tiled=True),
        down_block,
        preferred_element_type=jnp.float32,
    ).astype(jnp.bfloat16)
    returned = lax.all_to_all(
        results.reshape(expert_count, capacity, down_block.shape[1]),
        "ep",
        split_axis=0,
        concat_axis=0,
        tiled=True,
    ).reshape(slot_rows, down_block.shape[1])
    picked = (
        returned[slot_index]
        .reshape(tok_rows, choose_count, down_block.shape[1])
        .astype(jnp.float32)
    )
    weights = pair_weights(group_prob, pair_logits)
    expert_output = jnp.sum(picked * weights[:, :, None], axis=1).astype(jnp.bfloat16)
    return (mixed, expert_output)


def solution(mesh):
    in_specs = (
        P("ep", "tp"),
        P("ep", "tp"),
        P("ep", "tp"),
        P(None, "tp"),
        P(None, "tp"),
        P("ep", "tp"),
        P(),
        P("ep", None),
        P("ep"),
        P("ep", None),
        P("ep", None, "tp"),
        P("ep", None, "tp"),
        P("ep", None, "tp"),
    )
    out_specs = (P("ep", "tp"), P("ep", "tp"))
    return jax.shard_map(
        per_device, mesh=mesh, in_specs=in_specs, out_specs=out_specs, check_vma=False
    )
```

profile of v0, /device:TPU:0, one launch (start us, length us, event | category | flops | bytes accessed | tf_op | source)
XLA Modules:
  0.0 170.7 jit_solution(3366997663291530493)
XLA Ops:
  7.2 0.8 copy.17
  8.0 0.7 broadcast_multiply_fusion
  8.7 0.1 eq.22
  8.9 0.9 reduce-window.6
  9.8 0.2 slice_reduce_fusion
  10.2 0.1 mul.117
  10.4 1.1 fusion.22
  11.5 8.4 %psum.7 = f32[160]{0:T(256)S(1)} all-reduce(f32[160]{0:T(256)S(1)} %fusion.22), channel_id=1, replica_groups=mesh['ep'=8,'tp'=4] {'tp'}, use_global_device_ids=true, to_apply=%region_4.5 | all-reduce | flops 160 | bytes 1280 | tf_op jit(solution)/shard_map/psum | solution.py:75
  19.9 0.7 dynamic_slice.3
  20.6 1.1 fusion.24
  21.8 4.5 %scatter_custom_fusion = bf16[480,1024]{1,0:T(8,128)(2,1)S(1)} fusion(s32[320]{0:T(512)S(1)} %fusion.30, bf16[160,1024]{1,0:T(8,128)(2,1)S(1)} %fusion.24, s32[1024]{0:T(1024)S(1)} %pad_clamp_fusion.1, bf16[]{:T(256)} %constant.18.clone.1), kind=kCustom, calls=%fused_computation.30 | custom fusion | bytes 983042 | tf_op jit(solution)/shard_map/scatter | solution.py:79
  26.2 0.2 reshape.137
  26.4 30.1 %all_to_all.10 = bf16[8,60,1024]{2,1,0:T(8,128)(2,1)S(1)} all-to-all(bf16[8,60,1024]{2,1,0:T(8,128)(2,1)S(1)} %reshape.137), channel_id=1, replica_groups=mesh['ep'=8,'tp'=4] {'ep'}, dimensions={0} | all-to-all | bytes 1966080 | tf_op jit(solution)/shard_map/all_to_all | solution.py:80
  56.6 1.1 reshape.138
  57.8 32.1 %all-gather.6.cloned.1.call-done = bf16[480,4096]{1,0:T(8,128)(2,1)} async-done(((bf16[480,1024]{1,0:T(8,128)(2,1)}), bf16[480,4096]{1,0:T(8,128)(2,1)}) %all-gather.6.cloned.1.call-update) | async-done | bytes 3932176 | tf_op jit(solution)/shard_map/all_gather | solution.py:87
  89.9 5.7 %fusion.4 = f32[480,512]{1,0:T(8,128)S(1)} fusion(bf16[480,4096]{1,0:T(8,128)(2,1)} %all-gather.6.cloned.1.call-done, bf16[1,4096,512]{2,1,0:T(8,128)(2,1)} %param.23), kind=kOutput, calls=%fused_computation.7 | convolution fusion | flops 2013265920 | bytes 9109504 | tf_op jit(solution)/shard_map/dot_general | solution.py:88
  95.7 3.0 %fusion.12 = bf16[480,512]{1,0:T(8,128)(2,1)} fusion(bf16[480,4096]{1,0:T(8,128)(2,1)S(1)} %copy-done.7, bf16[1,4096,512]{2,1,0:T(8,128)(2,1)S(1)} %copy-done.6, f32[480,512]{1,0:T(8,128)S(1)} %fusion.4), kind=kOutput, calls=%fused_computation.13 | convolution fusion | flops 2014740480 | bytes 9601024 | tf_op jit(solution)/shard_map/dot_general | solution.py:89
  98.8 0.1 convert_multiply_fusion
  99.0 3.4 %collective-permute-start = (f32[2,512]{1,0:T(2,128)S(1)}, f32[2,512]{1,0:T(2,128)S(1)}, u32[]{:S(2)}, u32[]{:S(2)}) collective-permute-start(f32[2,512]{1,0:T(2,128)S(1)} %slice.48), channel_id=1, source_target_pairs={{0,4},{4,8},{8,12},{12,16},{16,20},{20,24},{24,28},{1,5},{5,9},{9,... | collective-permute-start | bytes 12296 | tf_op jit(solution)/shard_map/ppermute | solution.py:15
  102.4 1.3 collective-permute-done
  103.7 1.2 fusion.20
  104.9 15.8 %all-gather.8.cloned.1.call-done = bf16[480,2048]{1,0:T(8,128)(2,1)} async-done(((bf16[480,512]{1,0:T(8,128)(2,1)}), bf16[480,2048]{1,0:T(8,128)(2,1)}) %all-gather.8.cloned.1.call-update) | async-done | bytes 1966096 | tf_op jit(solution)/shard_map/all_gather | solution.py:92
  120.8 5.0 %fusion.6 = bf16[480,1024]{1,0:T(8,128)(2,1)S(1)} fusion(bf16[480,2048]{1,0:T(8,128)(2,1)} %all-gather.8.cloned.1.call-done, bf16[1,2048,1024]{2,1,0:T(8,128)(2,1)} %param.25), kind=kOutput, calls=%fused_computation.10 | convolution fusion | flops 2013757440 | bytes 7143424 | tf_op jit(solution)/shard_map/dot_general | solution.py:91
  125.8 1.2 reshape.139
  126.9 5.5 %all-to-all-start.1 = ((bf16[8,60,1024]{2,1,0:T(8,128)(2,1)}), bf16[8,60,1024]{2,1,0:T(8,128)(2,1)S(1)}, u32[]{:S(2)}, u32[]{:S(2)}) async-start(bf16[8,60,1024]{2,1,0:T(8,128)(2,1)} %reshape.139), calls=%async_computation.1 | async-start | bytes 2097152 | tf_op jit(solution)/shard_map/all_to_all | solution.py:96
  132.6 12.9 %all-gather.4.cloned.1.call-done = bf16[512,2048]{1,0:T(8,128)(2,1)} async-done(((bf16[512,512]{1,0:T(8,128)(2,1)}), bf16[512,2048]{1,0:T(8,128)(2,1)}) %all-gather.4.cloned.1.call-update) | async-done | bytes 2097168 | tf_op jit(solution)/shard_map/all_gather | solution.py:60
  145.5 6.1 %convolution_convert_fusion = bf16[512,1024]{1,0:T(8,128)(2,1)} fusion(bf16[512,2048]{1,0:T(8,128)(2,1)} %all-gather.4.cloned.1.call-done, bf16[2048,1024]{1,0:T(8,128)(2,1)} %param.17), kind=kOutput, calls=%fused_computation.9 | convolution fusion | flops 2148007936 | bytes 7340032 | tf_op jit(solution)/shard_map/dot_general | solution.py:59
  151.6 7.0 %all-to-all-done.1 = bf16[8,60,1024]{2,1,0:T(8,128)(2,1)S(1)} async-done(((bf16[8,60,1024]{2,1,0:T(8,128)(2,1)}), bf16[8,60,1024]{2,1,0:T(8,128)(2,1)S(1)}, u32[]{:S(2)}, u32[]{:S(2)}) %all-to-all-start.1) | async-done | bytes 983072 | tf_op jit(solution)/shard_map/all_to_all | solution.py:96
  158.6 0.2 reshape.140
  158.8 2.1 %gather_fusion = bf16[320,1024]{1,0:T(8,128)(2,1)S(1)} fusion(bf16[480,1024]{1,0:T(8,128)(2,1)S(1)} %reshape.140, s32[1024]{0:T(1024)S(1)} %pad_clamp_fusion), kind=kCustom, calls=%fused_computation.1 | custom fusion | bytes 1312000 | tf_op jit(solution)/shard_map/gather | solution.py:104
  160.9 0.8 reshape.142
  161.7 2.4 %multiply_reduce_fusion = bf16[160,1024]{1,0:T(8,128)(2,1)} fusion(f32[160,2,1024]{2,1,0:T(2,128)S(1)} %reshape.142, f32[160,2]{1,0:T(8,128)S(1)} %copy.18), kind=kLoop, calls=%fused_computation.12 | loop fusion | flops 491520 | bytes 1639680 | tf_op jit(solution)/shard_map/reduce_sum | solution.py:109
  (39 shorter events, 0.7 us)
Async XLA Ops:
  7.2 82.8 %all-gather.6.cloned.1.call-start = ((), (), s32[]{:S(2)}) async-start(), calls=%async_computation.3 | async-start | bytes 4915200 | tf_op jit(solution)/shard_map/all_gather | solution.py:87
  57.7 63.0 %all-gather.8.cloned.1.call-start = ((), (), s32[]{:S(2)}) async-start(), calls=%async_computation.4 | async-start | bytes 2457600 | tf_op jit(solution)/shard_map/all_gather | solution.py:92
  89.9 5.7 %copy-start.6 = (bf16[1,4096,512]{2,1,0:T(8,128)(2,1)S(1)}, bf16[1,4096,512]{2,1,0:T(8,128)(2,1)}, u32[]{:S(2)}) copy-start(bf16[1,4096,512]{2,1,0:T(8,128)(2,1)} %param.24) | copy-start | bytes 12582916
  89.9 5.8 %copy-start.7 = (bf16[480,4096]{1,0:T(8,128)(2,1)S(1)}, bf16[480,4096]{1,0:T(8,128)(2,1)}, u32[]{:S(2)}) copy-start(bf16[480,4096]{1,0:T(8,128)(2,1)} %all-gather.6.cloned.1.call-done) | copy-start | bytes 11796484
  95.7 3.1 %copy-start.1 = (bf16[512,512]{1,0:T(8,128)(2,1)S(1)}, bf16[512,512]{1,0:T(8,128)(2,1)}, u32[]{:S(2)}) copy-start(bf16[512,512]{1,0:T(8,128)(2,1)} %param.15) | copy-start | bytes 1572868
  95.7 3.1 %copy-start.2 = (bf16[512,512]{1,0:T(8,128)(2,1)S(1)}, bf16[512,512]{1,0:T(8,128)(2,1)}, u32[]{:S(2)}) copy-start(bf16[512,512]{1,0:T(8,128)(2,1)} %param.14) | copy-start | bytes 1572868
  95.7 6.7 %copy-start.3 = (f32[3,512]{1,0:T(4,128)S(1)}, f32[3,512]{1,0:T(4,128)}, u32[]{:S(2)}) copy-start(f32[3,512]{1,0:T(4,128)} %param.16) | copy-start | bytes 18436
  95.7 8.0 %copy-start = (bf16[512,512]{1,0:T(8,128)(2,1)S(1)}, bf16[512,512]{1,0:T(8,128)(2,1)}, u32[]{:S(2)}) copy-start(bf16[512,512]{1,0:T(8,128)(2,1)} %param.13) | copy-start | bytes 1572868
  98.8 46.7 %all-gather.4.cloned.1.call-start = ((), (), s32[]{:S(2)}) async-start(), calls=%async_computation.2 | async-start | bytes 2621440 | tf_op jit(solution)/shard_map/all_gather | solution.py:60
  99.0 4.7 %collective-permute-start = (f32[2,512]{1,0:T(2,128)S(1)}, f32[2,512]{1,0:T(2,128)S(1)}, u32[]{:S(2)}, u32[]{:S(2)}) collective-permute-start(f32[2,512]{1,0:T(2,128)S(1)} %slice.48), channel_id=1, source_target_pairs={{0,4},{4,8},{8,12},{12,16},{16,20},{20,24},{24,28},{1,5},{5,9},{9,... | collective-permute-start | bytes 12296 | tf_op jit(solution)/shard_map/ppermute | solution.py:15
  125.7 6.7 %copy-start.4 = (f32[160,2]{0,1:T(2,128)S(1)}, f32[160,2]{0,1:T(2,128)}, u32[]{:S(2)}) copy-start(f32[160,2]{0,1:T(2,128)} %param.22) | copy-start | bytes 3844
  125.8 6.7 %copy-start.5 = (f32[160]{0:T(256)S(1)}, f32[160]{0:T(256)}, u32[]{:S(2)}) copy-start(f32[160]{0:T(256)} %param.21) | copy-start | bytes 1924
  126.9 31.7 %all-to-all-start.1 = ((bf16[8,60,1024]{2,1,0:T(8,128)(2,1)}), bf16[8,60,1024]{2,1,0:T(8,128)(2,1)S(1)}, u32[]{:S(2)}, u32[]{:S(2)}) async-start(bf16[8,60,1024]{2,1,0:T(8,128)(2,1)} %reshape.139), calls=%async_computation.1 | async-start | bytes 2097152 | tf_op jit(solution)/shard_map/all_to_all | solution.py:96
Sparse Core Ops, SparseCore 0:
  57.8 32.0 all-gather.5
  98.9 21.8 all-gather.7
  122.9 22.5 all-gather.3
where the time goes:
time: 171 us
  waiting for transfers between devices  69.2 us (40%)
  blocking collectives  38.5 us (23%)
  matrix products  19.9 us (12%)
  between operations  14 us (8%)
  local copies, waits for them, and re-layouts  12.3 us (7%)
  starting transfers between devices  9 us (5%)
  other arithmetic  7.81 us (5%)
    all_gather x1, waiting for transfers between devices, per_device(): shard_piece = lax.all_gather(arrived, 'tp', axis=1, tiled=True)  32.1 us
    all_to_all x1, blocking collectives, per_device(): lax.all_to_all(buffer.reshape(expert_count, capacity, columns), 'ep', spl...  30.1 us
    all_gather x1, waiting for transfers between devices, per_device(): lax.all_gather(hidden, 'tp', axis=1, tiled=True)  15.8 us
    all_gather x1, waiting for transfers between devices, per_device(): lax.all_gather(mixer_rows, 'tp', axis=1, tiled=True)  12.9 us
    psum x1, blocking collectives, per_device(): squares = lax.psum(jnp.sum(features * features, axis=1), 'tp')  8.39 us
    all_to_all x1, waiting for transfers between devices, per_device(): lax.all_to_all(results.reshape(expert_count, capacity, down_block.shape[1...  6.98 us
    dot_general x1, matrix products, per_device(): jnp.dot(lax.all_gather(mixer_rows, 'tp', axis=1, tiled=True), mix_out_wei...  6.12 us
    dot_general x1, matrix products, per_device(): jnp.dot(shard_piece, gate_block, preferred_element_type=jnp.float32)  5.71 us
  transfers between devices with their start and end apart: 5, of which 5 were waited for; matrix products, arithmetic and copies ran while one was open for 8% of the time, Pallas kernels for 0%

commit v1 on v0

v1 whole, which is shorter than its diff:
```python
import jax
import jax.numpy as jnp
from jax import lax
from jax.sharding import PartitionSpec as P

D = 4096
EPS = 1e-06
CHUNKS = 1
PERMUTED = False


def shifted(block, axis, distance):
    devices = range(lax.axis_size(axis))
    route = [(i - distance, i) for i in devices if i - distance in devices]
    return lax.ppermute(block, axis, route)


def rotated(block, axis, distance):
    size = lax.axis_size(axis)
    return lax.ppermute(block, axis, [(i, (i + distance) % size) for i in range(size)])


def core_swapped(block):
    return lax.ppermute(block, "tp", [(i, i ^ 1) for i in range(lax.axis_size("tp"))])


def chip_rotated(block, distance):
    size = lax.axis_size("tp")
    return lax.ppermute(block, "tp", [(i, (i + 2 * distance) % size) for i in range(size)])


def pieces_over_tp(block):
    size = lax.axis_size("tp")
    own = lax.axis_index("tp")
    pieces = [(own, block), (own ^ 1, core_swapped(block))]
    for distance in range(1, size // 2):
        piece = chip_rotated(block, distance)
        source = (own - 2 * distance) % size
        pieces = pieces + [(source, piece), (source ^ 1, core_swapped(piece))]
    return pieces


def rows_of(weight, start, count):
    return lax.dynamic_slice_in_dim(weight, start, count, 0)


def summed_product(pieces, weight):
    total = None
    for source, piece in pieces:
        width = piece.shape[1]
        part = jnp.dot(
            piece, rows_of(weight, source * width, width), preferred_element_type=jnp.float32
        )
        total = part if total is None else total + part
    return total


def pair_weights(group_prob, pair_logits):
    spread = pair_logits[:, 0] - pair_logits[:, 1]
    return (
        jnp.stack([jax.nn.sigmoid(spread), jax.nn.sigmoid(-spread)], axis=1) * group_prob[:, None]
    )


def send_out(buffer, expert_count):
    rows, width = buffer.shape
    capacity = rows // expert_count
    if not PERMUTED:
        return lax.all_to_all(
            buffer.reshape(expert_count, capacity, width), "ep", 0, 0, tiled=True
        ).reshape(rows, width)
    blocks = [buffer[:capacity]]
    for j in range(1, expert_count):
        blocks.append(rotated(buffer[j * capacity : (j + 1) * capacity], "ep", j))
    return jnp.concatenate(blocks, axis=0)


def send_back(buffer, expert_count):
    rows, width = buffer.shape
    capacity = rows // expert_count
    if not PERMUTED:
        return send_out(buffer, expert_count)
    blocks = [buffer[:capacity]]
    for j in range(1, expert_count):
        blocks.append(rotated(buffer[j * capacity : (j + 1) * capacity], "ep", -j))
    return jnp.concatenate(blocks, axis=0)


def per_device(
    conv_gate,
    conv_in_gate,
    conv_value,
    conv_taps,
    mix_out_weight,
    expert_input,
    expert_gain,
    routes,
    group_prob,
    pair_logits,
    expert_gate,
    expert_up,
    expert_down,
):
    reach = conv_taps.shape[0] - 1
    token_rows = conv_value.shape[0]
    expert_count = lax.axis_size("ep")
    tok_rows, choose_count = routes.shape
    capacity = 3 * tok_rows * choose_count // (2 * expert_count)
    capacity = -(-capacity // 8) * 8
    slot_rows = expert_count * capacity

    experts = jnp.arange(expert_count, dtype=jnp.int32)
    if PERMUTED:
        experts = (experts + lax.axis_index("ep")) % expert_count
    member = (routes[:, None, :] == experts[None, :, None]).astype(jnp.float32)
    named = jnp.sum(member, axis=2)
    token = jnp.arange(tok_rows, dtype=jnp.int32)
    before = (token[None, :] < token[:, None]).astype(jnp.bfloat16)
    earlier = jnp.dot(before, named.astype(jnp.bfloat16), preferred_element_type=jnp.float32)
    place = jnp.where(named > 0, earlier, -1.0)
    slot = jnp.arange(capacity, dtype=jnp.int32).astype(jnp.float32)
    chosen = (place.T[:, None, :] == slot[None, :, None]).reshape(slot_rows, tok_rows)
    chosen = chosen.astype(jnp.bfloat16)

    gate_block = expert_gate[0]
    up_block = expert_up[0]
    down_block = expert_down[0]
    columns = expert_input.shape[1]
    span = columns // CHUNKS
    gate_sum = None
    up_sum = None
    squares = None
    for chunk in range(CHUNKS):
        part = expert_input[:, chunk * span : (chunk + 1) * span]
        buffer = jnp.dot(chosen, part, preferred_element_type=jnp.float32).astype(jnp.bfloat16)
        arrived = send_out(buffer, expert_count)
        for source, piece in pieces_over_tp(arrived):
            start = source * columns + chunk * span
            features = piece.astype(jnp.float32)
            piece_squares = jnp.sum(features * features, axis=1)
            gained = (features * rows_of(expert_gain, start, span)[None, :]).astype(jnp.bfloat16)
            gate_part = jnp.dot(
                gained, rows_of(gate_block, start, span), preferred_element_type=jnp.float32
            )
            up_part = jnp.dot(
                gained, rows_of(up_block, start, span), preferred_element_type=jnp.float32
            )
            if squares is None:
                gate_sum, up_sum, squares = gate_part, up_part, piece_squares
            else:
                gate_sum = gate_sum + gate_part
                up_sum = up_sum + up_part
                squares = squares + piece_squares
    scale = lax.rsqrt(squares / D + EPS)[:, None]
    hidden = (jax.nn.silu(gate_sum * scale) * (up_sum * scale)).astype(jnp.bfloat16)
    results = summed_product(pieces_over_tp(hidden), down_block).astype(jnp.bfloat16)
    returned = send_back(results, expert_count)

    products = conv_in_gate.astype(jnp.float32) * conv_value.astype(jnp.float32)
    earlier_rows = shifted(products[token_rows - reach :], "ep", 1)
    padded = jnp.concatenate([earlier_rows, products], axis=0)
    convolved = jnp.zeros_like(products)
    for offset in range(reach + 1):
        convolved = convolved + conv_taps[offset][None, :] * padded[offset : offset + token_rows]
    mixer_rows = (conv_gate.astype(jnp.float32) * convolved).astype(jnp.bfloat16)
    mixed = summed_product(pieces_over_tp(mixer_rows), mix_out_weight).astype(jnp.bfloat16)

    weights = pair_weights(group_prob, pair_logits)
    by_expert = jnp.sum(member * weights[:, None, :], axis=2)
    spread_weights = (
        (place[:, :, None] == slot[None, None, :]).astype(jnp.float32) * by_expert[:, :, None]
    ).reshape(tok_rows, slot_rows)
    high = lax.reduce_precision(spread_weights, 8, 7)
    low = (spread_weights - high).astype(jnp.bfloat16)
    expert_output = (
        jnp.dot(high.astype(jnp.bfloat16), returned, preferred_element_type=jnp.float32)
        + jnp.dot(low, returned, preferred_element_type=jnp.float32)
    ).astype(jnp.bfloat16)
    return (mixed, expert_output)


def solution(mesh):
    in_specs = (
        P("ep", "tp"),
        P("ep", "tp"),
        P("ep", "tp"),
        P(None, "tp"),
        P(None, "tp"),
        P("ep", "tp"),
        P(),
        P("ep", None),
        P("ep"),
        P("ep", None),
        P("ep", None, "tp"),
        P("ep", None, "tp"),
        P("ep", None, "tp"),
    )
    out_specs = (P("ep", "tp"), P("ep", "tp"))
    return jax.shard_map(
        per_device, mesh=mesh, in_specs=in_specs, out_specs=out_specs, check_vma=False
    )
```

time: 171 us -> 118 us (0.69)
  waiting for transfers between devices: 69.2 us -> 42.7 us
  between operations: 14 us -> 0.98 us
  local copies, waits for them, and re-layouts: 12.3 us -> 1.38 us
  blocking collectives: 38.5 us -> 32.8 us
  starting transfers between devices: 9 us -> 12.8 us
  other arithmetic: 7.81 us -> 5 us
    all_gather x3 -> x0, waiting for transfers between devices: 60.8 us -> none  [the longest x1 32.1 us: per_device(): shard_piece = lax.all_gather(arrived, 'tp', axis=1, tiled=True)]
    ppermute x0 -> x9, waiting for transfers between devices: none -> 34.5 us  [the longest x3 33.6 us: chip_rotated(): lax.ppermute(block, 'tp', [(i, (i + 2 * distance) % size) for i in range(...]
    psum x1 -> x0, blocking collectives: 8.39 us -> none  [per_device(): squares = lax.psum(jnp.sum(features * features, axis=1), 'tp')]
    ppermute x0 -> x9, starting transfers between devices: none -> 4.81 us  [the longest x3 4.72 us: chip_rotated(): lax.ppermute(block, 'tp', [(i, (i + 2 * distance) % size) for i in range(...]
    scatter x1 -> x0, local copies, waits for them, and re-layouts: 4.49 us -> none  [per_device(): jnp.zeros((slot_rows, columns), jnp.bfloat16).at[slot_index]]
    all_to_all x1, blocking collectives: 30.1 us -> 32.8 us  [send_out(): lax.all_to_all(buffer.reshape(expert_count, capacity, width), 'ep', 0, 0,...]
    reshape x4 -> x0, local copies, waits for them, and re-layouts: 2.64 us -> none  [the longest x1 1.16 us: per_device(): results.reshape(expert_count, capacity, down_block.shape[1])]
    gather x1 -> x0, local copies, waits for them, and re-layouts: 2.09 us -> none  [per_device(): returned[slot_index].reshape(tok_rows, choose_count, down_block.shape[1])]
  transfers between devices with their start and end apart: 5 -> 11, of which waited for: 5 -> 6; matrix products, arithmetic and copies ran while one was open for 8% -> 17% of each run, Pallas kernels for 0% -> 0%
where the time goes in v1:
time: 118 us; the launch traced here: 117 us
  waiting for transfers between devices  42.7 us (36%)
  blocking collectives  32.8 us (28%)
  matrix products  21.4 us (18%)
  starting transfers between devices  12.8 us (11%)
  other arithmetic  5 us (4%)
  local copies, waits for them, and re-layouts  1.38 us (1%)
    ppermute x3, waiting for transfers between devices, chip_rotated(): lax.ppermute(block, 'tp', [(i, (i + 2 * distance) % size) for i in range(...  33.6 us
    all_to_all x1, blocking collectives, send_out(): lax.all_to_all(buffer.reshape(expert_count, capacity, width), 'ep', 0, 0,...  32.8 us
    dot_general x8, matrix products, summed_product(): jnp.dot(piece, rows_of(weight, source * width, width), preferred_element_...  10.3 us
    all_to_all x1, waiting for transfers between devices, send_out(): lax.all_to_all(buffer.reshape(expert_count, capacity, width), 'ep', 0, 0,...  8.23 us
    ppermute x3, starting transfers between devices, chip_rotated(): lax.ppermute(block, 'tp', [(i, (i + 2 * distance) % size) for i in range(...  4.72 us
    all_to_all x1, starting transfers between devices, send_out(): lax.all_to_all(buffer.reshape(expert_count, capacity, width), 'ep', 0, 0,...  4.54 us
    dot_general x4, matrix products, per_device(): jnp.dot(gained, rows_of(gate_block, start, span), preferred_element_type=...  4.53 us
    dot_general x4, matrix products, per_device(): jnp.dot(gained, rows_of(up_block, start, span), preferred_element_type=jn...  4.42 us
  transfers between devices with their start and end apart: 11, of which 6 were waited for; matrix products, arithmetic and copies ran while one was open for 17% of the time, Pallas kernels for 0%

profile of v1, /device:TPU:0, one launch (start us, length us, event | category | flops | bytes accessed | tf_op | source)
XLA Modules:
  0.0 117.2 jit_solution(16570187442814220710)
XLA Ops:
  0.7 0.8 add_divide_fusion.1
  1.5 0.7 maximum_multiply_fusion
  2.1 0.7 select_reduce_fusion
  3.7 32.8 %all_to_all.10 = bf16[8,64,1024]{2,1,0:T(8,128)(2,1)S(1)} all-to-all(bf16[8,64,1024]{2,1,0:T(8,128)(2,1)S(1)} %bitcast.72), channel_id=1, replica_groups=mesh['ep'=8,'tp'=4] {'ep'}, dimensions={0} | all-to-all | bytes 2097152 | tf_op jit(solution)/shard_map/all_to_all | solution.py:69
  36.5 1.5 %collective-permute-start.5 = (bf16[512,1024]{1,0:T(8,128)(2,1)S(1)}, bf16[512,1024]{1,0:T(8,128)(2,1)S(1)}, u32[]{:S(2)}, u32[]{:S(2)}) collective-permute-start(bf16[512,1024]{1,0:T(8,128)(2,1)S(1)} %bitcast.70), channel_id=1, source_target_pairs={{0,2},{1,3},{2,0},{3,1},{4,6},{5,7},{6,4},{7,5},{8,10},{9,11},{10,... | collective-permute-start | bytes 3145736 | tf_op jit(solution)/shard_map/ppermute | solution.py:29
  38.1 1.3 %fusion.1 = (f32[8,64]{1,0:T(8,128)S(1)}, bf16[8,64,1024]{2,1,0:T(8,128)(2,1)}) fusion(bf16[8,64,1024]{2,1,0:T(8,128)(2,1)S(1)} %all_to_all.10, f32[1024]{0:T(1024)S(1)} %get-tuple-element.10), kind=kLoop, calls=%fused_computation.9 | loop fusion | flops 2620928 | bytes 2103296 | tf_op jit(solution)/shard_map/reduce_sum | solution.py:140
  39.4 2.3 %fusion.34 = f32[512,512]{1,0:T(8,128)S(1)} fusion(bf16[512,1024]{1,0:T(8,128)(2,1)} %bitcast.73, bf16[1,4096,512]{2,1,0:T(8,128)(2,1)} %param.23, s32[]{:T(128)S(6)} %select_n.62), kind=kOutput, calls=%fused_computation.57 | convolution fusion | flops 536870912 | bytes 3145732 | tf_op jit(solution)/shard_map/dot_general | solution.py:142
  41.8 2.1 %fusion.29 = f32[512,512]{1,0:T(8,128)S(1)} fusion(bf16[512,1024]{1,0:T(8,128)(2,1)S(1)} %bitcast.74, bf16[1,4096,512]{2,1,0:T(8,128)(2,1)} %param.24, s32[]{:T(128)S(6)} %select_n.62), kind=kOutput, calls=%fused_computation.52 | convolution fusion | flops 536870912 | bytes 3145732 | tf_op jit(solution)/shard_map/dot_general | solution.py:145
  43.9 16.4 %collective-permute-done.5 = bf16[512,1024]{1,0:T(8,128)(2,1)S(1)} collective-permute-done((bf16[512,1024]{1,0:T(8,128)(2,1)S(1)}, bf16[512,1024]{1,0:T(8,128)(2,1)S(1)}, u32[]{:S(2)}, u32[]{:S(2)}) %collective-permute-start.5) | collective-permute-done | bytes 1048608 | tf_op jit(solution)/shard_map/ppermute | solution.py:29
  60.6 0.7 convolution_add_fusion.5
  61.6 1.2 copy-done.10
  62.7 0.7 convolution_add_fusion.2
  63.5 0.7 convolution_add_fusion.4
  64.2 0.7 convolution_add_fusion.1
  65.3 0.7 fusion.9
  66.0 0.9 multiply_convert_fusion
  66.9 1.6 %collective-permute-start.8 = (bf16[512,512]{1,0:T(8,128)(2,1)S(1)}, bf16[512,512]{1,0:T(8,128)(2,1)S(1)}, u32[]{:S(2)}, u32[]{:S(2)}) collective-permute-start(bf16[512,512]{1,0:T(8,128)(2,1)S(1)} %multiply_convert_fusion), channel_id=1, source_target_pairs={{0,2},{1,3},{2,0},{3,1},{4,6},{5,7},{6,4},{7,5},{8,10},{9,11},{10,... | collective-permute-start | bytes 1572872 | tf_op jit(solution)/shard_map/ppermute | solution.py:29
  68.7 3.4 %collective-permute-start = (f32[2,512]{1,0:T(2,128)S(1)}, f32[2,512]{1,0:T(2,128)S(1)}, u32[]{:S(2)}, u32[]{:S(2)}) collective-permute-start(f32[2,512]{1,0:T(2,128)S(1)} %slice.32), channel_id=1, source_target_pairs={{0,4},{4,8},{8,12},{12,16},{16,20},{20,24},{24,28},{1,5},{5,9},{9,... | collective-permute-start | bytes 12296 | tf_op jit(solution)/shard_map/ppermute | solution.py:15
  72.2 2.1 %fusion.24 = f32[512,1024]{1,0:T(8,128)S(1)} fusion(bf16[512,512]{1,0:T(8,128)(2,1)S(1)} %multiply_convert_fusion, bf16[1,2048,1024]{2,1,0:T(8,128)(2,1)} %param.25, s32[]{:T(128)S(6)} %select_n.55), kind=kOutput, calls=%fused_computation.47 | convolution fusion | flops 536870912 | bytes 3670020 | tf_op jit(solution)/shard_map/dot_general | solution.py:51
  74.3 7.0 %collective-permute-done.8 = bf16[512,512]{1,0:T(8,128)(2,1)S(1)} collective-permute-done((bf16[512,512]{1,0:T(8,128)(2,1)S(1)}, bf16[512,512]{1,0:T(8,128)(2,1)S(1)}, u32[]{:S(2)}, u32[]{:S(2)}) %collective-permute-start.8) | collective-permute-done | bytes 524320 | tf_op jit(solution)/shard_map/ppermute | solution.py:29
  81.3 0.7 fusion.20
  82.1 0.7 fusion.22
  83.2 1.7 %add_convert_fusion = bf16[512,1024]{1,0:T(8,128)(2,1)} fusion(f32[512,1024]{1,0:T(8,128)S(1)} %fusion.20, f32[512,1024]{1,0:T(8,128)S(1)} %fusion.24, f32[512,1024]{1,0:T(8,128)S(1)} %fusion.22, bf16[512,512]{1,0:T(8,128)(2,1)S(1)} %collective-permute-done.9, bf16[1,2048,1024]{2,1,0:T(8,128)(2,1)S(1)} %copy-done.1, s32[]{:T(128)S(6)} %select_n.59), kind=kOutput, calls=%fused_computation.16 | convolution fusion | flops 538968064 | bytes 8912900 | tf_op jit(solution)/shard_map/dot_general | solution.py:51
  85.0 4.5 %all-to-all-start.1 = ((bf16[8,64,1024]{2,1,0:T(8,128)(2,1)}), bf16[8,64,1024]{2,1,0:T(8,128)(2,1)S(1)}, u32[]{:S(2)}, u32[]{:S(2)}) async-start(bf16[8,64,1024]{2,1,0:T(8,128)(2,1)} %bitcast.20), calls=%async_computation.1 | async-start | bytes 2097152 | tf_op jit(solution)/shard_map/all_to_all | solution.py:69
  90.0 1.6 %collective-permute-start.2 = (bf16[512,512]{1,0:T(8,128)(2,1)S(1)}, bf16[512,512]{1,0:T(8,128)(2,1)S(1)}, u32[]{:S(2)}, u32[]{:S(2)}) collective-permute-start(bf16[512,512]{1,0:T(8,128)(2,1)S(1)} %fusion.17), channel_id=1, source_target_pairs={{0,2},{1,3},{2,0},{3,1},{4,6},{5,7},{6,4},{7,5},{8,10},{9,11},{10,... | collective-permute-start | bytes 1572872 | tf_op jit(solution)/shard_map/ppermute | solution.py:29
  91.5 1.9 %fusion.53 = f32[512,1024]{1,0:T(8,128)S(1)} fusion(bf16[512,512]{1,0:T(8,128)(2,1)S(1)} %fusion.17, bf16[2048,1024]{1,0:T(8,128)(2,1)} %param.17, s32[]{:T(128)S(6)} %select_n.55), kind=kOutput, calls=%fused_computation.77 | convolution fusion | flops 536870912 | bytes 3670020 | tf_op jit(solution)/shard_map/dot_general | solution.py:51
  93.5 10.2 %collective-permute-done.2 = bf16[512,512]{1,0:T(8,128)(2,1)S(1)} collective-permute-done((bf16[512,512]{1,0:T(8,128)(2,1)S(1)}, bf16[512,512]{1,0:T(8,128)(2,1)S(1)}, u32[]{:S(2)}, u32[]{:S(2)}) %collective-permute-start.2) | collective-permute-done | bytes 524320 | tf_op jit(solution)/shard_map/ppermute | solution.py:29
  103.7 0.7 fusion.49
  104.4 0.7 fusion.51
  105.6 1.7 %add_convert_fusion.1 = bf16[512,1024]{1,0:T(8,128)(2,1)} fusion(f32[512,1024]{1,0:T(8,128)S(1)} %fusion.49, f32[512,1024]{1,0:T(8,128)S(1)} %fusion.53, f32[512,1024]{1,0:T(8,128)S(1)} %fusion.51, bf16[512,512]{1,0:T(8,128)(2,1)S(1)} %collective-permute-done.3, bf16[2048,1024]{1,0:T(8,128)(2,1)S(1)} %copy-done.2, s32[]{:T(128)S(6)} %select_n.59), kind=kOutput, calls=%fused_computation.17 | convolution fusion | flops 538968064 | bytes 8912900 | tf_op jit(solution)/shard_map/dot_general | solution.py:51
  107.3 8.2 %all-to-all-done.1 = bf16[8,64,1024]{2,1,0:T(8,128)(2,1)S(1)} async-done(((bf16[8,64,1024]{2,1,0:T(8,128)(2,1)}), bf16[8,64,1024]{2,1,0:T(8,128)(2,1)S(1)}, u32[]{:S(2)}, u32[]{:S(2)}) %all-to-all-start.1) | async-done | bytes 1048608 | tf_op jit(solution)/shard_map/all_to_all | solution.py:69
  116.0 1.2 fusion.11
  (52 shorter events, 3.8 us)
Async XLA Ops:
  0.6 2.6 %copy-start = (bf16[160,1024]{1,0:T(8,128)(2,1)S(1)}, bf16[160,1024]{1,0:T(8,128)(2,1)}, u32[]{:S(2)}) copy-start(bf16[160,1024]{1,0:T(8,128)(2,1)} %param.18) | copy-start | bytes 983044
  0.6 37.4 %copy-start.8 = (f32[4096]{0:T(1024)S(1)}, f32[4096]{0:T(1024)}, u32[]{:S(2)}) copy-start(f32[4096]{0:T(1024)} %param.19) | copy-start | bytes 49156
  36.5 23.7 %collective-permute-start.5 = (bf16[512,1024]{1,0:T(8,128)(2,1)S(1)}, bf16[512,1024]{1,0:T(8,128)(2,1)S(1)}, u32[]{:S(2)}, u32[]{:S(2)}) collective-permute-start(bf16[512,1024]{1,0:T(8,128)(2,1)S(1)} %bitcast.70), channel_id=1, source_target_pairs={{0,2},{1,3},{2,0},{3,1},{4,6},{5,7},{6,4},{7,5},{8,10},{9,11},{10,... | collective-permute-start | bytes 3145736 | tf_op jit(solution)/shard_map/ppermute | solution.py:29
  38.1 22.5 %collective-permute-start.4 = (bf16[512,1024]{1,0:T(8,128)(2,1)S(1)}, bf16[512,1024]{1,0:T(8,128)(2,1)S(1)}, u32[]{:S(2)}, u32[]{:S(2)}) collective-permute-start(bf16[512,1024]{1,0:T(8,128)(2,1)S(1)} %bitcast.71), channel_id=1, source_target_pairs={{0,1},{1,0},{2,3},{3,2},{4,5},{5,4},{6,7},{7,6},{8,9},{9,8},{10,11... | collective-permute-start | bytes 3145736 | tf_op jit(solution)/shard_map/ppermute | solution.py:24
  39.4 2.3 %copy-start.3 = (bf16[8,64,1024]{2,1,0:T(8,128)(2,1)S(1)}, bf16[8,64,1024]{2,1,0:T(8,128)(2,1)}, u32[]{:S(2)}) copy-start(bf16[8,64,1024]{2,1,0:T(8,128)(2,1)} %get-tuple-element.7) | copy-start | bytes 3145732
  41.8 18.8 %copy-start.7 = (bf16[1,4096,512]{2,1,0:T(8,128)(2,1)S(1)}, bf16[1,4096,512]{2,1,0:T(8,128)(2,1)}, u32[]{:S(2)}) copy-start(bf16[1,4096,512]{2,1,0:T(8,128)(2,1)} %param.23) | copy-start | bytes 12582916
  60.2 4.7 %collective-permute-start.6 = (bf16[512,1024]{1,0:T(8,128)(2,1)S(1)}, bf16[512,1024]{1,0:T(8,128)(2,1)S(1)}, u32[]{:S(2)}, u32[]{:S(2)}) collective-permute-start(bf16[512,1024]{1,0:T(8,128)(2,1)S(1)} %collective-permute-done.5), channel_id=1, source_target_pairs={{0,1},{1,0},{2,3},{3,2},{4,5},{5,4},{6,7},{7,6},{8,9},{9,8},{10,11... | collective-permute-start | bytes 3145736 | tf_op jit(solution)/shard_map/ppermute | solution.py:24
  60.5 2.2 %copy-start.10 = (bf16[1,4096,512]{2,1,0:T(8,128)(2,1)S(1)}, bf16[1,4096,512]{2,1,0:T(8,128)(2,1)}, u32[]{:S(2)}) copy-start(bf16[1,4096,512]{2,1,0:T(8,128)(2,1)} %param.24) | copy-start | bytes 12582916
  66.0 2.5 %copy-start.5 = (bf16[512,512]{1,0:T(8,128)(2,1)S(1)}, bf16[512,512]{1,0:T(8,128)(2,1)}, u32[]{:S(2)}) copy-start(bf16[512,512]{1,0:T(8,128)(2,1)} %param.15) | copy-start | bytes 1572868
  66.0 2.5 %copy-start.6 = (bf16[512,512]{1,0:T(8,128)(2,1)S(1)}, bf16[512,512]{1,0:T(8,128)(2,1)}, u32[]{:S(2)}) copy-start(bf16[512,512]{1,0:T(8,128)(2,1)} %param.14) | copy-start | bytes 1572868
  66.9 14.4 %collective-permute-start.8 = (bf16[512,512]{1,0:T(8,128)(2,1)S(1)}, bf16[512,512]{1,0:T(8,128)(2,1)S(1)}, u32[]{:S(2)}, u32[]{:S(2)}) collective-permute-start(bf16[512,512]{1,0:T(8,128)(2,1)S(1)} %multiply_convert_fusion), channel_id=1, source_target_pairs={{0,2},{1,3},{2,0},{3,1},{4,6},{5,7},{6,4},{7,5},{8,10},{9,11},{10,... | collective-permute-start | bytes 1572872 | tf_op jit(solution)/shard_map/ppermute | solution.py:29
  68.7 20.8 %collective-permute-start = (f32[2,512]{1,0:T(2,128)S(1)}, f32[2,512]{1,0:T(2,128)S(1)}, u32[]{:S(2)}, u32[]{:S(2)}) collective-permute-start(f32[2,512]{1,0:T(2,128)S(1)} %slice.32), channel_id=1, source_target_pairs={{0,4},{4,8},{8,12},{12,16},{16,20},{20,24},{24,28},{1,5},{5,9},{9,... | collective-permute-start | bytes 12296 | tf_op jit(solution)/shard_map/ppermute | solution.py:15
  72.1 9.2 %copy-start.1 = (bf16[1,2048,1024]{2,1,0:T(8,128)(2,1)S(1)}, bf16[1,2048,1024]{2,1,0:T(8,128)(2,1)}, u32[]{:S(2)}) copy-start(bf16[1,2048,1024]{2,1,0:T(8,128)(2,1)} %param.25) | copy-start | bytes 12582916
  72.2 9.9 %collective-permute-start.7 = (bf16[512,512]{1,0:T(8,128)(2,1)S(1)}, bf16[512,512]{1,0:T(8,128)(2,1)S(1)}, u32[]{:S(2)}, u32[]{:S(2)}) collective-permute-start(bf16[512,512]{1,0:T(8,128)(2,1)S(1)} %multiply_convert_fusion), channel_id=1, source_target_pairs={{0,1},{1,0},{2,3},{3,2},{4,5},{5,4},{6,7},{7,6},{8,9},{9,8},{10,11... | collective-permute-start | bytes 1572872 | tf_op jit(solution)/shard_map/ppermute | solution.py:24
  81.3 1.9 %collective-permute-start.9 = (bf16[512,512]{1,0:T(8,128)(2,1)S(1)}, bf16[512,512]{1,0:T(8,128)(2,1)S(1)}, u32[]{:S(2)}, u32[]{:S(2)}) collective-permute-start(bf16[512,512]{1,0:T(8,128)(2,1)S(1)} %collective-permute-done.8), channel_id=1, source_target_pairs={{0,1},{1,0},{2,3},{3,2},{4,5},{5,4},{6,7},{7,6},{8,9},{9,8},{10,11... | collective-permute-start | bytes 1572872 | tf_op jit(solution)/shard_map/ppermute | solution.py:24
  84.9 4.5 %copy-start.9 = (f32[3,512]{1,0:T(4,128)S(1)}, f32[3,512]{1,0:T(4,128)}, u32[]{:S(2)}) copy-start(f32[3,512]{1,0:T(4,128)} %param.16) | copy-start | bytes 18436
  85.0 4.6 %copy-start.4 = (bf16[512,512]{1,0:T(8,128)(2,1)S(1)}, bf16[512,512]{1,0:T(8,128)(2,1)}, u32[]{:S(2)}) copy-start(bf16[512,512]{1,0:T(8,128)(2,1)} %param.13) | copy-start | bytes 1572868
  85.0 30.6 %all-to-all-start.1 = ((bf16[8,64,1024]{2,1,0:T(8,128)(2,1)}), bf16[8,64,1024]{2,1,0:T(8,128)(2,1)S(1)}, u32[]{:S(2)}, u32[]{:S(2)}) async-start(bf16[8,64,1024]{2,1,0:T(8,128)(2,1)} %bitcast.20), calls=%async_computation.1 | async-start | bytes 2097152 | tf_op jit(solution)/shard_map/all_to_all | solution.py:69
  89.9 13.8 %copy-start.2 = (bf16[2048,1024]{1,0:T(8,128)(2,1)S(1)}, bf16[2048,1024]{1,0:T(8,128)(2,1)}, u32[]{:S(2)}) copy-start(bf16[2048,1024]{1,0:T(8,128)(2,1)} %param.17) | copy-start | bytes 12582916
  90.0 13.7 %collective-permute-start.2 = (bf16[512,512]{1,0:T(8,128)(2,1)S(1)}, bf16[512,512]{1,0:T(8,128)(2,1)S(1)}, u32[]{:S(2)}, u32[]{:S(2)}) collective-permute-start(bf16[512,512]{1,0:T(8,128)(2,1)S(1)} %fusion.17), channel_id=1, source_target_pairs={{0,2},{1,3},{2,0},{3,1},{4,6},{5,7},{6,4},{7,5},{8,10},{9,11},{10,... | collective-permute-start | bytes 1572872 | tf_op jit(solution)/shard_map/ppermute | solution.py:29
  91.5 12.9 %collective-permute-start.1 = (bf16[512,512]{1,0:T(8,128)(2,1)S(1)}, bf16[512,512]{1,0:T(8,128)(2,1)S(1)}, u32[]{:S(2)}, u32[]{:S(2)}) collective-permute-start(bf16[512,512]{1,0:T(8,128)(2,1)S(1)} %fusion.17), channel_id=1, source_target_pairs={{0,1},{1,0},{2,3},{3,2},{4,5},{5,4},{6,7},{7,6},{8,9},{9,8},{10,11... | collective-permute-start | bytes 1572872 | tf_op jit(solution)/shard_map/ppermute | solution.py:24
  103.7 1.9 %collective-permute-start.3 = (bf16[512,512]{1,0:T(8,128)(2,1)S(1)}, bf16[512,512]{1,0:T(8,128)(2,1)S(1)}, u32[]{:S(2)}, u32[]{:S(2)}) collective-permute-start(bf16[512,512]{1,0:T(8,128)(2,1)S(1)} %collective-permute-done.2), channel_id=1, source_target_pairs={{0,1},{1,0},{2,3},{3,2},{4,5},{5,4},{6,7},{7,6},{8,9},{9,8},{10,11... | collective-permute-start | bytes 1572872 | tf_op jit(solution)/shard_map/ppermute | solution.py:24

commit v2 on v1

--- a/solution.py
+++ b/solution.py
@@ -5,7 +5,6 @@
 
 D = 4096
 EPS = 1e-06
-CHUNKS = 1
 PERMUTED = False
 
 
@@ -126,31 +125,39 @@
     up_block = expert_up[0]
     down_block = expert_down[0]
     columns = expert_input.shape[1]
-    span = columns // CHUNKS
-    gate_sum = None
-    up_sum = None
-    squares = None
-    for chunk in range(CHUNKS):
-        part = expert_input[:, chunk * span : (chunk + 1) * span]
+    lanes = 128
+    first = max(lanes, columns * 4 // 8 // lanes * lanes)
+    spans = [(0, first), (first, columns - first)] if first < columns else [(0, columns)]
+    dispatched = []
+    for begin, span in spans:
+        part = expert_input[:, begin : begin + span]
         buffer = jnp.dot(chosen, part, preferred_element_type=jnp.float32).astype(jnp.bfloat16)
-        arrived = send_out(buffer, expert_count)
-        for source, piece in pieces_over_tp(arrived):
-            start = source * columns + chunk * span
-            features = piece.astype(jnp.float32)
-            piece_squares = jnp.sum(features * features, axis=1)
-            gained = (features * rows_of(expert_gain, start, span)[None, :]).astype(jnp.bfloat16)
-            gate_part = jnp.dot(
-                gained, rows_of(gate_block, start, span), preferred_element_type=jnp.float32
-            )
-            up_part = jnp.dot(
-                gained, rows_of(up_block, start, span), preferred_element_type=jnp.float32
-            )
-            if squares is None:
-                gate_sum, up_sum, squares = gate_part, up_part, piece_squares
-            else:
-                gate_sum = gate_sum + gate_part
-                up_sum = up_sum + up_part
-                squares = squares + piece_squares
+        dispatched.append(send_out(buffer, expert_count))
+
+    def added(sums, source, piece, begin):
+        start, span = source * columns + begin, piece.shape[1]
+        features = piece.astype(jnp.float32)
+        gained = (features * rows_of(expert_gain, start, span)[None, :]).astype(jnp.bfloat16)
+        parts = (
+            jnp.dot(gained, rows_of(gate_block, start, span), preferred_element_type=jnp.float32),
+            jnp.dot(gained, rows_of(up_block, start, span), preferred_element_type=jnp.float32),
+            jnp.sum(features * features, axis=1),
+        )
+        return parts if sums is None else tuple(a + b for a, b in zip(sums, parts))
+
+    sums = None
+    later = []
+    for number, (begin, span) in enumerate(spans):
+        arrived = dispatched[number]
+        if number > 0:
+            arrived, sums = lax.optimization_barrier((arrived, sums))
+        pieces = pieces_over_tp(arrived)
+        for source, piece in pieces[:2]:
+            sums = added(sums, source, piece, begin)
+        later = later + [(source, piece, begin) for source, piece in pieces[2:]]
+    for source, piece, begin in later:
+        sums = added(sums, source, piece, begin)
+    gate_sum, up_sum, squares = sums
     scale = lax.rsqrt(squares / D + EPS)[:, None]
     hidden = (jax.nn.silu(gate_sum * scale) * (up_sum * scale)).astype(jnp.bfloat16)
     results = summed_product(pieces_over_tp(hidden), down_block).astype(jnp.bfloat16)

time: 118 us -> 114 us (0.966)
  blocking collectives: 32.8 us -> 0 us
  starting transfers between devices: 12.8 us -> 26.7 us
  matrix products: 21.4 us -> 31.1 us
  waiting for transfers between devices: 42.7 us -> 48.7 us
    all_to_all x1 -> x0, blocking collectives: 32.8 us -> none  [send_out(): lax.all_to_all(buffer.reshape(expert_count, capacity, width), 'ep', 0, 0,...]
    all_to_all x1 -> x3, waiting for transfers between devices: 8.23 us -> 25.5 us  [send_out(): lax.all_to_all(buffer.reshape(expert_count, capacity, width), 'ep', 0, 0,...]
    all_to_all x1 -> x3, starting transfers between devices: 4.54 us -> 16 us  [send_out(): lax.all_to_all(buffer.reshape(expert_count, capacity, width), 'ep', 0, 0,...]
    ppermute x3 -> x4, waiting for transfers between devices: 33.6 us -> 22.4 us  [chip_rotated(): lax.ppermute(block, 'tp', [(i, (i + 2 * distance) % size) for i in range(...]
    dot_general x8 -> x16, matrix products: 8.95 us -> 15.1 us  [the longest x8 8.21 us: added(): jnp.dot(gained, rows_of(gate_block, start, span), preferred_element_type=...]
    dot_general x1 -> x2, matrix products: 0.43 us -> 4.02 us  [per_device(): jnp.dot(chosen, part, preferred_element_type=jnp.float32)]
    ppermute x3 -> x4, starting transfers between devices: 4.72 us -> 6.2 us  [chip_rotated(): lax.ppermute(block, 'tp', [(i, (i + 2 * distance) % size) for i in range(...]
  transfers between devices with their start and end apart: 11 -> 16, of which waited for: 6 -> 8; matrix products, arithmetic and copies ran while one was open for 17% -> 26% of each run, Pallas kernels for 0% -> 0%
where the time goes in v2:
time: 114 us; the launch traced here: 113 us
  waiting for transfers between devices  48.7 us (43%)
  matrix products  31.1 us (27%)
  starting transfers between devices  26.7 us (23%)
  other arithmetic  4.36 us (4%)
    all_to_all x3, waiting for transfers between devices, send_out(): lax.all_to_all(buffer.reshape(expert_count, capacity, width), 'ep', 0, 0,...  25.5 us
    ppermute x4, waiting for transfers between devices, chip_rotated(): lax.ppermute(block, 'tp', [(i, (i + 2 * distance) % size) for i in range(...  22.4 us
    all_to_all x3, starting transfers between devices, send_out(): lax.all_to_all(buffer.reshape(expert_count, capacity, width), 'ep', 0, 0,...  16 us
    dot_general x8, matrix products, summed_product(): jnp.dot(piece, rows_of(weight, source * width, width), preferred_element_...  10.3 us
    dot_general x8, matrix products, added(): jnp.dot(gained, rows_of(gate_block, start, span), preferred_element_type=...  8.21 us
    dot_general x8, matrix products, added(): jnp.dot(gained, rows_of(up_block, start, span), preferred_element_type=jn...  6.86 us
    ppermute x4, starting transfers between devices, chip_rotated(): lax.ppermute(block, 'tp', [(i, (i + 2 * distance) % size) for i in range(...  6.2 us
    dot_general x2, matrix products, per_device(): jnp.dot(chosen, part, preferred_element_type=jnp.float32)  4.02 us
  transfers between devices with their start and end apart: 16, of which 8 were waited for; matrix products, arithmetic and copies ran while one was open for 26% of the time, Pallas kernels for 0%

profile of v2, /device:TPU:0, one launch (start us, length us, event | category | flops | bytes accessed | tf_op | source)
XLA Modules:
  0.0 113.1 jit_solution(14059464895457228051)
XLA Ops:
  0.6 0.8 add_divide_fusion.1
  3.2 2.0 %convolution_convert_fusion = bf16[512,512]{1,0:T(8,128)(2,1)} fusion(pred[512,160]{1,0:T(32,128)(4,1)S(1)} %bitcast_compare_fusion, bf16[160,1024]{1,0:T(8,128)(2,1)} %param.18), kind=kOutput, calls=%fused_computation.36 | convolution fusion | flops 84148224 | bytes 770048 | tf_op jit(solution)/shard_map/dot_general | solution.py:134
  5.2 7.3 %all-to-all-start.1 = ((bf16[8,64,512]{2,1,0:T(8,128)(2,1)}), bf16[8,64,512]{2,1,0:T(8,128)(2,1)S(1)}, u32[]{:S(2)}, u32[]{:S(2)}) async-start(bf16[8,64,512]{2,1,0:T(8,128)(2,1)} %bitcast.7), calls=%async_computation.1 | async-start | bytes 1048576 | tf_op jit(solution)/shard_map/all_to_all | solution.py:68
  12.5 0.9 fusion.142
  13.4 2.0 %convolution_convert_fusion.1 = bf16[512,512]{1,0:T(8,128)(2,1)} fusion(pred[512,160]{1,0:T(32,128)(4,1)S(1)} %bitcast_compare_fusion, bf16[160,1024]{1,0:T(8,128)(2,1)} %param.18), kind=kOutput, calls=%fused_computation.37 | convolution fusion | flops 84148224 | bytes 770048 | tf_op jit(solution)/shard_map/dot_general | solution.py:134
  15.4 11.6 %all-to-all-done.1 = bf16[8,64,512]{2,1,0:T(8,128)(2,1)S(1)} async-done(((bf16[8,64,512]{2,1,0:T(8,128)(2,1)}), bf16[8,64,512]{2,1,0:T(8,128)(2,1)S(1)}, u32[]{:S(2)}, u32[]{:S(2)}) %all-to-all-start.1) | async-done | bytes 524320 | tf_op jit(solution)/shard_map/all_to_all | solution.py:68
  27.0 3.6 %all-to-all-start = ((bf16[8,64,512]{2,1,0:T(8,128)(2,1)}), bf16[8,64,512]{2,1,0:T(8,128)(2,1)S(1)}, u32[]{:S(2)}, u32[]{:S(2)}) async-start(bf16[8,64,512]{2,1,0:T(8,128)(2,1)} %bitcast.5), calls=%async_computation | async-start | bytes 1048576 | tf_op jit(solution)/shard_map/all_to_all | solution.py:68
  30.6 1.6 %collective-permute-start.6 = (bf16[512,512]{1,0:T(8,128)(2,1)S(1)}, bf16[512,512]{1,0:T(8,128)(2,1)S(1)}, u32[]{:S(2)}, u32[]{:S(2)}) collective-permute-start(bf16[512,512]{1,0:T(8,128)(2,1)S(1)} %bitcast.102), channel_id=1, source_target_pairs={{0,2},{1,3},{2,0},{3,1},{4,6},{5,7},{6,4},{7,5},{8,10},{9,11},{10,... | collective-permute-start | bytes 1572872 | tf_op jit(solution)/shard_map/ppermute | solution.py:28
  32.5 1.5 %fusion.69 = f32[512,512]{1,0:T(8,128)S(1)} fusion(bf16[512,512]{1,0:T(8,128)(2,1)S(1)} %bitcast.99, bf16[1,4096,512]{2,1,0:T(8,128)(2,1)} %param.24, s32[]{:T(128)S(6)} %select_n.84), kind=kOutput, calls=%fused_computation.108 | convolution fusion | flops 268435456 | bytes 2097156 | tf_op jit(solution)/shard_map/dot_general | solution.py:143
  34.0 1.5 %fusion.72 = f32[512,512]{1,0:T(8,128)S(1)} fusion(bf16[512,512]{1,0:T(8,128)(2,1)S(1)} %bitcast.100, bf16[1,4096,512]{2,1,0:T(8,128)(2,1)} %param.23, s32[]{:T(128)S(6)} %select_n.84), kind=kOutput, calls=%fused_computation.111 | convolution fusion | flops 268435456 | bytes 2097156 | tf_op jit(solution)/shard_map/dot_general | solution.py:142
  35.7 1.5 %convolution_add_fusion.8 = f32[512,512]{1,0:T(8,128)S(1)} fusion(f32[512,512]{1,0:T(8,128)S(1)} %fusion.69, bf16[1,4096,512]{2,1,0:T(8,128)(2,1)} %param.24, s32[]{:T(128)S(6)} %select_n.85, bf16[512,512]{1,0:T(8,128)(2,1)S(1)} %collective-permute-done.4, f32[512]{0:T(512)S(1)} %get-tuple-element.21), kind=kOutput, calls=%fused_computation.17 | convolution fusion | flops 269484032 | bytes 3147780 | tf_op jit(solution)/shard_map/dot_general | solution.py:143
  37.2 2.5 %convolution_add_fusion.9 = f32[512,512]{1,0:T(8,128)} fusion(f32[512,512]{1,0:T(8,128)S(1)} %fusion.72, bf16[1,4096,512]{2,1,0:T(8,128)(2,1)} %param.23, s32[]{:T(128)S(6)} %select_n.85, bf16[512,512]{1,0:T(8,128)(2,1)S(1)} %collective-permute-done.4, f32[512]{0:T(512)S(1)} %get-tuple-element.21), kind=kOutput, calls=%fused_computation.18 | convolution fusion | flops 269484032 | bytes 3147780 | tf_op jit(solution)/shard_map/dot_general | solution.py:142
  39.6 5.7 %all-to-all-done = bf16[8,64,512]{2,1,0:T(8,128)(2,1)S(1)} async-done(((bf16[8,64,512]{2,1,0:T(8,128)(2,1)}), bf16[8,64,512]{2,1,0:T(8,128)(2,1)S(1)}, u32[]{:S(2)}, u32[]{:S(2)}) %all-to-all-start) | async-done | bytes 524320 | tf_op jit(solution)/shard_map/all_to_all | solution.py:68
  45.3 1.5 %collective-permute-start.8 = (bf16[512,512]{1,0:T(8,128)(2,1)S(1)}, bf16[512,512]{1,0:T(8,128)(2,1)S(1)}, u32[]{:S(2)}, u32[]{:S(2)}) collective-permute-start(bf16[512,512]{1,0:T(8,128)(2,1)S(1)} %bitcast.94), channel_id=1, source_target_pairs={{0,2},{1,3},{2,0},{3,1},{4,6},{5,7},{6,4},{7,5},{8,10},{9,11},{10,... | collective-permute-start | bytes 1572872 | tf_op jit(solution)/shard_map/ppermute | solution.py:28
  46.8 2.0 %convolution_add_fusion.7 = f32[512,512]{1,0:T(8,128)S(1)} fusion(f32[512,512]{1,0:T(8,128)} %convolution_add_fusion.9, bf16[1,4096,512]{2,1,0:T(8,128)(2,1)} %param.23, s32[]{:T(128)S(6)} %select_n.86, bf16[512,512]{1,0:T(8,128)(2,1)S(1)} %bitcast.96, f32[512]{0:T(512)S(1)} %get-tuple-element.20), kind=kOutput, calls=%fused_computation.16 | convolution fusion | flops 269484032 | bytes 3147780 | tf_op jit(solution)/shard_map/dot_general | solution.py:142
  48.8 1.5 %convolution_add_fusion.3 = f32[512,512]{1,0:T(8,128)S(1)} fusion(f32[512,512]{1,0:T(8,128)S(1)} %convolution_add_fusion.8, bf16[1,4096,512]{2,1,0:T(8,128)(2,1)} %param.24, s32[]{:T(128)S(6)} %select_n.86, bf16[512,512]{1,0:T(8,128)(2,1)S(1)} %bitcast.97, f32[512]{0:T(512)S(1)} %get-tuple-element.20), kind=kOutput, calls=%fused_computation.9 | convolution fusion | flops 269484032 | bytes 3147780 | tf_op jit(solution)/shard_map/dot_general | solution.py:143
  52.2 5.6 %collective-permute-done.8 = bf16[512,512]{1,0:T(8,128)(2,1)S(1)} collective-permute-done((bf16[512,512]{1,0:T(8,128)(2,1)S(1)}, bf16[512,512]{1,0:T(8,128)(2,1)S(1)}, u32[]{:S(2)}, u32[]{:S(2)}) %collective-permute-start.8) | collective-permute-done | bytes 524320 | tf_op jit(solution)/shard_map/ppermute | solution.py:28
  62.3 1.5 %collective-permute-start.11 = (bf16[512,512]{1,0:T(8,128)(2,1)S(1)}, bf16[512,512]{1,0:T(8,128)(2,1)S(1)}, u32[]{:S(2)}, u32[]{:S(2)}) collective-permute-start(bf16[512,512]{1,0:T(8,128)(2,1)S(1)} %fusion.7), channel_id=1, source_target_pairs={{0,2},{1,3},{2,0},{3,1},{4,6},{5,7},{6,4},{7,5},{8,10},{9,11},{10,... | collective-permute-start | bytes 1572872 | tf_op jit(solution)/shard_map/ppermute | solution.py:28
  64.1 3.9 %collective-permute-start = (f32[2,512]{1,0:T(2,128)S(1)}, f32[2,512]{1,0:T(2,128)S(1)}, u32[]{:S(2)}, u32[]{:S(2)}) collective-permute-start(f32[2,512]{1,0:T(2,128)S(1)} %slice.40), channel_id=1, source_target_pairs={{0,4},{4,8},{8,12},{12,16},{16,20},{20,24},{24,28},{1,5},{5,9},{9,... | collective-permute-start | bytes 12296 | tf_op jit(solution)/shard_map/ppermute | solution.py:14
  68.1 2.1 %fusion.38 = f32[512,1024]{1,0:T(8,128)S(1)} fusion(bf16[512,512]{1,0:T(8,128)(2,1)S(1)} %fusion.7, bf16[1,2048,1024]{2,1,0:T(8,128)(2,1)} %param.25, s32[]{:T(128)S(6)} %select_n.77), kind=kOutput, calls=%fused_computation.74 | convolution fusion | flops 536870912 | bytes 3670020 | tf_op jit(solution)/shard_map/dot_general | solution.py:50
  70.2 6.6 %collective-permute-done.11 = bf16[512,512]{1,0:T(8,128)(2,1)S(1)} collective-permute-done((bf16[512,512]{1,0:T(8,128)(2,1)S(1)}, bf16[512,512]{1,0:T(8,128)(2,1)S(1)}, u32[]{:S(2)}, u32[]{:S(2)}) %collective-permute-start.11) | collective-permute-done | bytes 524320 | tf_op jit(solution)/shard_map/ppermute | solution.py:28
  77.5 0.7 fusion.36
  78.6 1.7 %add_convert_fusion = bf16[512,1024]{1,0:T(8,128)(2,1)} fusion(f32[512,1024]{1,0:T(8,128)S(1)} %fusion.34, f32[512,1024]{1,0:T(8,128)S(1)} %fusion.38, f32[512,1024]{1,0:T(8,128)S(1)} %fusion.36, bf16[512,512]{1,0:T(8,128)(2,1)S(1)} %collective-permute-done.12, bf16[1,2048,1024]{2,1,0:T(8,128)(2,1)S(1)} %copy-done, s32[]{:T(128)S(6)} %select_n.81), kind=kOutput, calls=%fused_computation | convolution fusion | flops 538968064 | bytes 8912900 | tf_op jit(solution)/shard_map/dot_general | solution.py:50
  80.3 5.1 %all-to-all-start.2 = ((bf16[8,64,1024]{2,1,0:T(8,128)(2,1)}), bf16[8,64,1024]{2,1,0:T(8,128)(2,1)S(1)}, u32[]{:S(2)}, u32[]{:S(2)}) async-start(bf16[8,64,1024]{2,1,0:T(8,128)(2,1)} %bitcast.30), calls=%async_computation.2 | async-start | bytes 2097152 | tf_op jit(solution)/shard_map/all_to_all | solution.py:68
  85.9 1.6 %collective-permute-start.2 = (bf16[512,512]{1,0:T(8,128)(2,1)S(1)}, bf16[512,512]{1,0:T(8,128)(2,1)S(1)}, u32[]{:S(2)}, u32[]{:S(2)}) collective-permute-start(bf16[512,512]{1,0:T(8,128)(2,1)S(1)} %fusion.15), channel_id=1, source_target_pairs={{0,2},{1,3},{2,0},{3,1},{4,6},{5,7},{6,4},{7,5},{8,10},{9,11},{10,... | collective-permute-start | bytes 1572872 | tf_op jit(solution)/shard_map/ppermute | solution.py:28
  87.4 1.9 %fusion.49 = f32[512,1024]{1,0:T(8,128)S(1)} fusion(bf16[512,512]{1,0:T(8,128)(2,1)S(1)} %fusion.15, bf16[2048,1024]{1,0:T(8,128)(2,1)} %param.17, s32[]{:T(128)S(6)} %select_n.77), kind=kOutput, calls=%fused_computation.85 | convolution fusion | flops 536870912 | bytes 3670020 | tf_op jit(solution)/shard_map/dot_general | solution.py:50
  89.4 10.3 %collective-permute-done.2 = bf16[512,512]{1,0:T(8,128)(2,1)S(1)} collective-permute-done((bf16[512,512]{1,0:T(8,128)(2,1)S(1)}, bf16[512,512]{1,0:T(8,128)(2,1)S(1)}, u32[]{:S(2)}, u32[]{:S(2)}) %collective-permute-start.2) | collective-permute-done | bytes 524320 | tf_op jit(solution)/shard_map/ppermute | solution.py:28
  99.6 0.7 fusion.45
  100.4 0.7 fusion.47
  101.5 1.7 %add_convert_fusion.1 = bf16[512,1024]{1,0:T(8,128)(2,1)} fusion(f32[512,1024]{1,0:T(8,128)S(1)} %fusion.45, f32[512,1024]{1,0:T(8,128)S(1)} %fusion.49, f32[512,1024]{1,0:T(8,128)S(1)} %fusion.47, bf16[512,512]{1,0:T(8,128)(2,1)S(1)} %collective-permute-done.3, bf16[2048,1024]{1,0:T(8,128)(2,1)S(1)} %copy-done.1, s32[]{:T(128)S(6)} %select_n.81), kind=kOutput, calls=%fused_computation.1 | convolution fusion | flops 538968064 | bytes 8912900 | tf_op jit(solution)/shard_map/dot_general | solution.py:50
  103.3 8.2 %all-to-all-done.2 = bf16[8,64,1024]{2,1,0:T(8,128)(2,1)S(1)} async-done(((bf16[8,64,1024]{2,1,0:T(8,128)(2,1)}), bf16[8,64,1024]{2,1,0:T(8,128)(2,1)S(1)}, u32[]{:S(2)}, u32[]{:S(2)}) %all-to-all-start.2) | async-done | bytes 1048608 | tf_op jit(solution)/shard_map/all_to_all | solution.py:68
  111.9 1.2 %fusion.9 = bf16[160,1024]{1,0:T(8,128)(2,1)} fusion(f32[160,1024]{1,0:T(8,128)S(1)} %convolution_bitcast_fusion, bf16[8,64,1024]{2,1,0:T(8,128)(2,1)S(1)} %all-to-all-done.2, f32[160,8]{0,1:T(8,128)S(1)} %get-tuple-element.10, f32[160,8]{0,1:T(8,128)S(1)} %convolution_select_fusion, f32[64]{0:T(128)S(1)} %iota_convert_fusion), kind=kOutput, calls=%fused_computation.41 | convolution fusion | flops 168427520 | bytes 2042112 | tf_op jit(solution)/shard_map/dot_general | solution.py:183
  (69 shorter events, 11.4 us)
Async XLA Ops:
  5.2 21.8 %all-to-all-start.1 = ((bf16[8,64,512]{2,1,0:T(8,128)(2,1)}), bf16[8,64,512]{2,1,0:T(8,128)(2,1)S(1)}, u32[]{:S(2)}, u32[]{:S(2)}) async-start(bf16[8,64,512]{2,1,0:T(8,128)(2,1)} %bitcast.7), calls=%async_computation.1 | async-start | bytes 1048576 | tf_op jit(solution)/shard_map/all_to_all | solution.py:68
  27.0 18.3 %all-to-all-start = ((bf16[8,64,512]{2,1,0:T(8,128)(2,1)}), bf16[8,64,512]{2,1,0:T(8,128)(2,1)S(1)}, u32[]{:S(2)}, u32[]{:S(2)}) async-start(bf16[8,64,512]{2,1,0:T(8,128)(2,1)} %bitcast.5), calls=%async_computation | async-start | bytes 1048576 | tf_op jit(solution)/shard_map/all_to_all | solution.py:68
  30.6 4.9 %collective-permute-start.4 = (bf16[512,512]{1,0:T(8,128)(2,1)S(1)}, bf16[512,512]{1,0:T(8,128)(2,1)S(1)}, u32[]{:S(2)}, u32[]{:S(2)}) collective-permute-start(bf16[512,512]{1,0:T(8,128)(2,1)S(1)} %bitcast.101), channel_id=1, source_target_pairs={{0,1},{1,0},{2,3},{3,2},{4,5},{5,4},{6,7},{7,6},{8,9},{9,8},{10,11... | collective-permute-start | bytes 1572872 | tf_op jit(solution)/shard_map/ppermute | solution.py:23
  30.6 19.7 %collective-permute-start.6 = (bf16[512,512]{1,0:T(8,128)(2,1)S(1)}, bf16[512,512]{1,0:T(8,128)(2,1)S(1)}, u32[]{:S(2)}, u32[]{:S(2)}) collective-permute-start(bf16[512,512]{1,0:T(8,128)(2,1)S(1)} %bitcast.102), channel_id=1, source_target_pairs={{0,2},{1,3},{2,0},{3,1},{4,6},{5,7},{6,4},{7,5},{8,10},{9,11},{10,... | collective-permute-start | bytes 1572872 | tf_op jit(solution)/shard_map/ppermute | solution.py:28
  45.3 5.6 %copy-start.2 = (bf16[1,4096,512]{2,1,0:T(8,128)(2,1)S(1)}, bf16[1,4096,512]{2,1,0:T(8,128)(2,1)}, u32[]{:S(2)}) copy-start(bf16[1,4096,512]{2,1,0:T(8,128)(2,1)} %param.23) | copy-start | bytes 12582916
  45.3 12.4 %collective-permute-start.8 = (bf16[512,512]{1,0:T(8,128)(2,1)S(1)}, bf16[512,512]{1,0:T(8,128)(2,1)S(1)}, u32[]{:S(2)}, u32[]{:S(2)}) collective-permute-start(bf16[512,512]{1,0:T(8,128)(2,1)S(1)} %bitcast.94), channel_id=1, source_target_pairs={{0,2},{1,3},{2,0},{3,1},{4,6},{5,7},{6,4},{7,5},{8,10},{9,11},{10,... | collective-permute-start | bytes 1572872 | tf_op jit(solution)/shard_map/ppermute | solution.py:28
  46.8 11.1 %collective-permute-start.5 = (bf16[512,512]{1,0:T(8,128)(2,1)S(1)}, bf16[512,512]{1,0:T(8,128)(2,1)S(1)}, u32[]{:S(2)}, u32[]{:S(2)}) collective-permute-start(bf16[512,512]{1,0:T(8,128)(2,1)S(1)} %bitcast.95), channel_id=1, source_target_pairs={{0,1},{1,0},{2,3},{3,2},{4,5},{5,4},{6,7},{7,6},{8,9},{9,8},{10,11... | collective-permute-start | bytes 1572872 | tf_op jit(solution)/shard_map/ppermute | solution.py:23
  46.8 4.9 %copy-start.3 = (bf16[1,4096,512]{2,1,0:T(8,128)(2,1)S(1)}, bf16[1,4096,512]{2,1,0:T(8,128)(2,1)}, u32[]{:S(2)}) copy-start(bf16[1,4096,512]{2,1,0:T(8,128)(2,1)} %param.24) | copy-start | bytes 12582916
  50.3 7.8 %collective-permute-start.7 = (bf16[512,512]{1,0:T(8,128)(2,1)S(1)}, bf16[512,512]{1,0:T(8,128)(2,1)S(1)}, u32[]{:S(2)}, u32[]{:S(2)}) collective-permute-start(bf16[512,512]{1,0:T(8,128)(2,1)S(1)} %collective-permute-done.6), channel_id=1, source_target_pairs={{0,1},{1,0},{2,3},{3,2},{4,5},{5,4},{6,7},{7,6},{8,9},{9,8},{10,11... | collective-permute-start | bytes 1572872 | tf_op jit(solution)/shard_map/ppermute | solution.py:23
  57.7 3.3 %collective-permute-start.9 = (bf16[512,512]{1,0:T(8,128)(2,1)S(1)}, bf16[512,512]{1,0:T(8,128)(2,1)S(1)}, u32[]{:S(2)}, u32[]{:S(2)}) collective-permute-start(bf16[512,512]{1,0:T(8,128)(2,1)S(1)} %collective-permute-done.8), channel_id=1, source_target_pairs={{0,1},{1,0},{2,3},{3,2},{4,5},{5,4},{6,7},{7,6},{8,9},{9,8},{10,11... | collective-permute-start | bytes 1572872 | tf_op jit(solution)/shard_map/ppermute | solution.py:23
  61.7 2.2 %copy-start.5 = (bf16[512,512]{1,0:T(8,128)(2,1)S(1)}, bf16[512,512]{1,0:T(8,128)(2,1)}, u32[]{:S(2)}) copy-start(bf16[512,512]{1,0:T(8,128)(2,1)} %param.15) | copy-start | bytes 1572868
  61.7 2.1 %copy-start.6 = (bf16[512,512]{1,0:T(8,128)(2,1)S(1)}, bf16[512,512]{1,0:T(8,128)(2,1)}, u32[]{:S(2)}) copy-start(bf16[512,512]{1,0:T(8,128)(2,1)} %param.14) | copy-start | bytes 1572868
  62.3 14.4 %collective-permute-start.11 = (bf16[512,512]{1,0:T(8,128)(2,1)S(1)}, bf16[512,512]{1,0:T(8,128)(2,1)S(1)}, u32[]{:S(2)}, u32[]{:S(2)}) collective-permute-start(bf16[512,512]{1,0:T(8,128)(2,1)S(1)} %fusion.7), channel_id=1, source_target_pairs={{0,2},{1,3},{2,0},{3,1},{4,6},{5,7},{6,4},{7,5},{8,10},{9,11},{10,... | collective-permute-start | bytes 1572872 | tf_op jit(solution)/shard_map/ppermute | solution.py:28
  64.1 21.4 %collective-permute-start = (f32[2,512]{1,0:T(2,128)S(1)}, f32[2,512]{1,0:T(2,128)S(1)}, u32[]{:S(2)}, u32[]{:S(2)}) collective-permute-start(f32[2,512]{1,0:T(2,128)S(1)} %slice.40), channel_id=1, source_target_pairs={{0,4},{4,8},{8,12},{12,16},{16,20},{20,24},{24,28},{1,5},{5,9},{9,... | collective-permute-start | bytes 12296 | tf_op jit(solution)/shard_map/ppermute | solution.py:14
  68.0 8.7 %copy-start = (bf16[1,2048,1024]{2,1,0:T(8,128)(2,1)S(1)}, bf16[1,2048,1024]{2,1,0:T(8,128)(2,1)}, u32[]{:S(2)}) copy-start(bf16[1,2048,1024]{2,1,0:T(8,128)(2,1)} %param.25) | copy-start | bytes 12582916
  68.0 9.4 %collective-permute-start.10 = (bf16[512,512]{1,0:T(8,128)(2,1)S(1)}, bf16[512,512]{1,0:T(8,128)(2,1)S(1)}, u32[]{:S(2)}, u32[]{:S(2)}) collective-permute-start(bf16[512,512]{1,0:T(8,128)(2,1)S(1)} %fusion.7), channel_id=1, source_target_pairs={{0,1},{1,0},{2,3},{3,2},{4,5},{5,4},{6,7},{7,6},{8,9},{9,8},{10,11... | collective-permute-start | bytes 1572872 | tf_op jit(solution)/shard_map/ppermute | solution.py:23
  76.7 1.9 %collective-permute-start.12 = (bf16[512,512]{1,0:T(8,128)(2,1)S(1)}, bf16[512,512]{1,0:T(8,128)(2,1)S(1)}, u32[]{:S(2)}, u32[]{:S(2)}) collective-permute-start(bf16[512,512]{1,0:T(8,128)(2,1)S(1)} %collective-permute-done.11), channel_id=1, source_target_pairs={{0,1},{1,0},{2,3},{3,2},{4,5},{5,4},{6,7},{7,6},{8,9},{9,8},{10,11... | collective-permute-start | bytes 1572872 | tf_op jit(solution)/shard_map/ppermute | solution.py:23
  78.2 7.2 %copy-start.7 = (f32[3,512]{1,0:T(4,128)S(1)}, f32[3,512]{1,0:T(4,128)}, u32[]{:S(2)}) copy-start(f32[3,512]{1,0:T(4,128)} %param.16) | copy-start | bytes 18436
  78.2 7.3 %copy-start.4 = (bf16[512,512]{1,0:T(8,128)(2,1)S(1)}, bf16[512,512]{1,0:T(8,128)(2,1)}, u32[]{:S(2)}) copy-start(bf16[512,512]{1,0:T(8,128)(2,1)} %param.13) | copy-start | bytes 1572868
  80.3 31.1 %all-to-all-start.2 = ((bf16[8,64,1024]{2,1,0:T(8,128)(2,1)}), bf16[8,64,1024]{2,1,0:T(8,128)(2,1)S(1)}, u32[]{:S(2)}, u32[]{:S(2)}) async-start(bf16[8,64,1024]{2,1,0:T(8,128)(2,1)} %bitcast.30), calls=%async_computation.2 | async-start | bytes 2097152 | tf_op jit(solution)/shard_map/all_to_all | solution.py:68
  85.4 14.2 %copy-start.1 = (bf16[2048,1024]{1,0:T(8,128)(2,1)S(1)}, bf16[2048,1024]{1,0:T(8,128)(2,1)}, u32[]{:S(2)}) copy-start(bf16[2048,1024]{1,0:T(8,128)(2,1)} %param.17) | copy-start | bytes 12582916
  85.9 13.8 %collective-permute-start.2 = (bf16[512,512]{1,0:T(8,128)(2,1)S(1)}, bf16[512,512]{1,0:T(8,128)(2,1)S(1)}, u32[]{:S(2)}, u32[]{:S(2)}) collective-permute-start(bf16[512,512]{1,0:T(8,128)(2,1)S(1)} %fusion.15), channel_id=1, source_target_pairs={{0,2},{1,3},{2,0},{3,1},{4,6},{5,7},{6,4},{7,5},{8,10},{9,11},{10,... | collective-permute-start | bytes 1572872 | tf_op jit(solution)/shard_map/ppermute | solution.py:28
  87.4 12.9 %collective-permute-start.1 = (bf16[512,512]{1,0:T(8,128)(2,1)S(1)}, bf16[512,512]{1,0:T(8,128)(2,1)S(1)}, u32[]{:S(2)}, u32[]{:S(2)}) collective-permute-start(bf16[512,512]{1,0:T(8,128)(2,1)S(1)} %fusion.15), channel_id=1, source_target_pairs={{0,1},{1,0},{2,3},{3,2},{4,5},{5,4},{6,7},{7,6},{8,9},{9,8},{10,11... | collective-permute-start | bytes 1572872 | tf_op jit(solution)/shard_map/ppermute | solution.py:23
  99.6 1.9 %collective-permute-start.3 = (bf16[512,512]{1,0:T(8,128)(2,1)S(1)}, bf16[512,512]{1,0:T(8,128)(2,1)S(1)}, u32[]{:S(2)}, u32[]{:S(2)}) collective-permute-start(bf16[512,512]{1,0:T(8,128)(2,1)S(1)} %collective-permute-done.2), channel_id=1, source_target_pairs={{0,1},{1,0},{2,3},{3,2},{4,5},{5,4},{6,7},{7,6},{8,9},{9,8},{10,11... | collective-permute-start | bytes 1572872 | tf_op jit(solution)/shard_map/ppermute | solution.py:23
